TPU v7x, 32 devices: a whole 2x2x4 slice. The times are simulated.
32 devices in a mesh: sp: 8 (over z, y), tp: 4 (over x, core).
Axes of the slice: x: 2, y: 2, z: 4, core: 2. Of those that a mesh axis runs over, the one named last changes fastest.
Arguments:
- tokens: bfloat16 [6, 2048, 2048], P(None, 'sp', 'tp'), may hold values from -6 to 6
- norm_gains: float32 [3, 2048], replicated, may hold values from 0.5 to 1.5
- weight_outer: bfloat16 [3, 2048, 1024], P(None, 'sp', 'tp'), may hold values from -0.125 to 0.125
- weight_inner: bfloat16 [3, 2048, 1024], P(None, 'sp', 'tp'), may hold values from -0.125 to 0.125
- weight_value: bfloat16 [3, 2048, 1024], P(None, 'sp', 'tp'), may hold values from -0.125 to 0.125
- conv_taps: bfloat16 [3, 3, 1024], P(None, None, 'tp'), may hold values from -3.5 to 3.5
- weight_output: bfloat16 [3, 1024, 2048], P(None, 'sp', 'tp'), may hold values from -0.1875 to 0.1875
Outputs:
- mixed_out: float32 [6, 2048, 2048], P(None, 'sp', 'tp')
All inputs are finite; a program needn't handle non-finite values.
Results may differ from a plain program's by a relative error of at most 0.03.
Values may be sent and summed in bfloat16 or wider, within the bound.
A program may use at most 128 MiB of HBM per device.

v0:
```python
import jax
import jax.numpy as jnp
from jax import lax
from jax.sharding import PartitionSpec as P

epsilon = 1e-06


def taken_in(array, axis, dim, take_in, carry):
    whole = jax.tree.map(lambda part: lax.all_gather(part, axis, axis=dim, tiled=True), array)
    return take_in(carry, whole, jnp.int32(0))


def from_behind(block, axis, distance):
    devices = range(lax.axis_size(axis))
    route = [(i - distance, i) for i in devices if i - distance in devices]
    return lax.ppermute(block, axis, route)


def normalize(values_in, gain_row):
    values = values_in.astype(jnp.float32)
    scale = lax.rsqrt(jnp.mean(values * values, axis=-1, keepdims=True) + epsilon)
    return (values * scale * gain_row.astype(jnp.float32)).astype(jnp.bfloat16)


def convolve(extended, taps):
    width = taps.shape[0]
    out_rows = extended.shape[1] - (width - 1)
    total = jnp.zeros((extended.shape[0], out_rows, extended.shape[2]), jnp.float32)
    for offset in range(width):
        total = total + taps[offset].astype(jnp.float32) * extended[:, offset : offset + out_rows]
    return total


def project_input(normed, pieces_in):
    empty = jnp.zeros((normed.shape[0], pieces_in[0].shape[1]), jnp.float32)

    def add_rows(totals, pieces, start):
        columns = lax.dynamic_slice_in_dim(normed, start, pieces[0].shape[0], 1)
        return tuple(
            (
                total + jnp.dot(columns, piece, preferred_element_type=jnp.float32)
                for total, piece in zip(totals, pieces)
            )
        )

    return taken_in(
        (pieces_in[0], pieces_in[1], pieces_in[2]), "sp", 0, add_rows, (empty, empty, empty)
    )


def project_output(flat_mix, piece_in):
    empty = jnp.zeros((flat_mix.shape[0], piece_in.shape[1]), jnp.float32)

    def add_rows(total, piece, start):
        columns = lax.dynamic_slice_in_dim(flat_mix, start, piece.shape[0], 1)
        return total + jnp.dot(columns, piece, preferred_element_type=jnp.float32)

    return taken_in(piece_in, "sp", 0, add_rows, empty)


def local(tokens, norm_gains, weight_outer, weight_inner, weight_value, conv_taps, weight_output):
    layers = conv_taps.shape[0]
    history = conv_taps.shape[1] - 1
    sequences = tokens.shape[0]
    current = tokens
    result = None
    for layer in range(layers):
        rows = current.shape[1]
        whole = lax.all_gather(current, "tp", axis=2, tiled=True)
        normed = normalize(whole, norm_gains[layer]).reshape(sequences * rows, whole.shape[2])
        outer, inner, value = project_input(
            normed, (weight_outer[layer], weight_inner[layer], weight_value[layer])
        )
        outer = outer.astype(jnp.bfloat16)
        inner = inner.astype(jnp.bfloat16)
        value = value.astype(jnp.bfloat16)
        outer, inner, value = lax.optimization_barrier((outer, inner, value))
        channels = outer.shape[1]
        outer = outer.reshape(sequences, rows, channels)
        gated = (inner.astype(jnp.float32) * value.astype(jnp.float32)).reshape(
            sequences, rows, channels
        )
        earlier = from_behind(gated[:, rows - history :], "sp", 1)
        extended = jnp.concatenate([earlier, gated], axis=1)
        kept = outer
        conved = convolve(extended, conv_taps[layer])
        mixer = (kept.astype(jnp.float32) * conved).astype(jnp.bfloat16)
        out_rows = mixer.shape[1]
        full_mix = lax.all_gather(mixer, "tp", axis=2, tiled=True)
        flat_mix = full_mix.reshape(sequences * out_rows, full_mix.shape[2])
        projected = project_output(flat_mix, weight_output[layer])
        result = projected.reshape(sequences, out_rows, projected.shape[1])
        current = result.astype(jnp.bfloat16)
    return result


def solution(mesh):
    placed = (
        P(None, "sp", "tp"),
        P(),
        P(None, "sp", "tp"),
        P(None, "sp", "tp"),
        P(None, "sp", "tp"),
        P(None, None, "tp"),
        P(None, "sp", "tp"),
    )
    return jax.shard_map(
        local, mesh=mesh, in_specs=placed, out_specs=P(None, "sp", "tp"), check_vma=False
    )
```

profile of v0, /device:TPU:0, one launch (start us, length us, event | category | flops | bytes accessed | tf_op | source)
XLA Modules:
  0.0 758.4 jit_solution(11629076176349233693)
XLA Ops:
  8.4 0.8 fusion.45
  9.2 0.7 fusion.46
  10.0 0.8 fusion.43
  10.9 47.0 %all-gather.31.cloned.1.call-done = bf16[6,256,2048]{2,1,0:T(8,128)(2,1)} async-done(((bf16[6,256,512]{2,1,0:T(8,128)(2,1)}), bf16[6,256,2048]{2,1,0:T(8,128)(2,1)}) %all-gather.31.cloned.1.call-update) | async-done | bytes 6291472 | tf_op jit(solution)/shard_map/all_gather | solution.py:70
  57.9 4.2 fusion
  62.5 4.2 fusion.2
  66.7 34.0 %all-gather.47.cloned.1.call-done = bf16[1,2048,256]{2,1,0:T(8,128)(2,1)} async-done(((bf16[1,256,256]{2,1,0:T(8,128)(2,1)}), bf16[1,2048,256]{2,1,0:T(8,128)(2,1)}) %all-gather.47.cloned.1.call-update) | async-done | bytes 1048592 | tf_op jit(solution)/shard_map/all_gather | solution.py:10
  100.7 4.8 convolution_convert_fusion.6
  105.5 36.4 %all-gather.45.cloned.1.call-done = bf16[1,2048,256]{2,1,0:T(8,128)(2,1)} async-done(((bf16[1,256,256]{2,1,0:T(8,128)(2,1)}), bf16[1,2048,256]{2,1,0:T(8,128)(2,1)}) %all-gather.45.cloned.1.call-update) | async-done | bytes 1048592 | tf_op jit(solution)/shard_map/all_gather | solution.py:10
  142.0 4.9 convolution_convert_fusion.7
  146.9 36.2 %all-gather.43.cloned.1.call-done = bf16[1,2048,256]{2,1,0:T(8,128)(2,1)} async-done(((bf16[1,256,256]{2,1,0:T(8,128)(2,1)}), bf16[1,2048,256]{2,1,0:T(8,128)(2,1)}) %all-gather.43.cloned.1.call-update) | async-done | bytes 1048592 | tf_op jit(solution)/shard_map/all_gather | solution.py:10
  183.1 4.8 convolution_convert_fusion.8
  188.1 2.3 collective-permute-start
  190.4 1.4 collective-permute-done
  191.8 1.5 fusion.26
  193.4 30.8 %all-gather.49.cloned.1.call-done = bf16[1,1024,512]{2,1,0:T(8,128)(2,1)} async-done(((bf16[1,128,512]{2,1,0:T(8,128)(2,1)}), bf16[1,1024,512]{2,1,0:T(8,128)(2,1)}) %all-gather.49.cloned.1.call-update) | async-done | bytes 1048592 | tf_op jit(solution)/shard_map/all_gather | solution.py:10
  224.2 28.8 %all-gather.33.cloned.1.call-done = bf16[6,256,1024]{2,1,0:T(8,128)(2,1)} async-done(((bf16[6,256,256]{2,1,0:T(8,128)(2,1)}), bf16[6,256,1024]{2,1,0:T(8,128)(2,1)}) %all-gather.33.cloned.1.call-update) | async-done | bytes 3145744 | tf_op jit(solution)/shard_map/all_gather | solution.py:90
  252.9 5.1 convolution_convert_fusion.10
  261.1 43.4 %all-gather.35.cloned.1.call-done = bf16[6,256,2048]{2,1,0:T(8,128)(2,1)} async-done(((bf16[6,256,512]{2,1,0:T(8,128)(2,1)}), bf16[6,256,2048]{2,1,0:T(8,128)(2,1)}) %all-gather.35.cloned.1.call-update) | async-done | bytes 6291472 | tf_op jit(solution)/shard_map/all_gather | solution.py:70
  304.5 4.2 fusion.3
  309.1 4.2 fusion.5
  313.3 34.0 %all-gather.55.cloned.1.call-done = bf16[1,2048,256]{2,1,0:T(8,128)(2,1)} async-done(((bf16[1,256,256]{2,1,0:T(8,128)(2,1)}), bf16[1,2048,256]{2,1,0:T(8,128)(2,1)}) %all-gather.55.cloned.1.call-update) | async-done | bytes 1048592 | tf_op jit(solution)/shard_map/all_gather | solution.py:10
  347.2 4.8 convolution_convert_fusion.3
  352.1 36.4 %all-gather.53.cloned.1.call-done = bf16[1,2048,256]{2,1,0:T(8,128)(2,1)} async-done(((bf16[1,256,256]{2,1,0:T(8,128)(2,1)}), bf16[1,2048,256]{2,1,0:T(8,128)(2,1)}) %all-gather.53.cloned.1.call-update) | async-done | bytes 1048592 | tf_op jit(solution)/shard_map/all_gather | solution.py:10
  388.5 4.8 convolution_convert_fusion.4
  393.4 36.3 %all-gather.51.cloned.1.call-done = bf16[1,2048,256]{2,1,0:T(8,128)(2,1)} async-done(((bf16[1,256,256]{2,1,0:T(8,128)(2,1)}), bf16[1,2048,256]{2,1,0:T(8,128)(2,1)}) %all-gather.51.cloned.1.call-update) | async-done | bytes 1048592 | tf_op jit(solution)/shard_map/all_gather | solution.py:10
  429.6 4.9 convolution_convert_fusion.5
  434.7 2.3 collective-permute-start.1
  437.0 1.4 collective-permute-done.1
  438.4 1.5 fusion.20
  440.0 30.9 %all-gather.57.cloned.1.call-done = bf16[1,1024,512]{2,1,0:T(8,128)(2,1)} async-done(((bf16[1,128,512]{2,1,0:T(8,128)(2,1)}), bf16[1,1024,512]{2,1,0:T(8,128)(2,1)}) %all-gather.57.cloned.1.call-update) | async-done | bytes 1048592 | tf_op jit(solution)/shard_map/all_gather | solution.py:10
  470.9 28.8 %all-gather.37.cloned.1.call-done = bf16[6,256,1024]{2,1,0:T(8,128)(2,1)} async-done(((bf16[6,256,256]{2,1,0:T(8,128)(2,1)}), bf16[6,256,1024]{2,1,0:T(8,128)(2,1)}) %all-gather.37.cloned.1.call-update) | async-done | bytes 3145744 | tf_op jit(solution)/shard_map/all_gather | solution.py:90
  499.7 5.1 convolution_convert_fusion.9
  507.4 43.8 %all-gather.39.cloned.1.call-done = bf16[6,256,2048]{2,1,0:T(8,128)(2,1)} async-done(((bf16[6,256,512]{2,1,0:T(8,128)(2,1)}), bf16[6,256,2048]{2,1,0:T(8,128)(2,1)}) %all-gather.39.cloned.1.call-update) | async-done | bytes 6291472 | tf_op jit(solution)/shard_map/all_gather | solution.py:70
  551.2 4.2 fusion.6
  555.8 4.2 fusion.8
  560.0 33.8 %all-gather.63.cloned.1.call-done = bf16[1,2048,256]{2,1,0:T(8,128)(2,1)} async-done(((bf16[1,256,256]{2,1,0:T(8,128)(2,1)}), bf16[1,2048,256]{2,1,0:T(8,128)(2,1)}) %all-gather.63.cloned.1.call-update) | async-done | bytes 1048592 | tf_op jit(solution)/shard_map/all_gather | solution.py:10
  593.8 4.8 convolution_convert_fusion
  598.7 36.3 %all-gather.61.cloned.1.call-done = bf16[1,2048,256]{2,1,0:T(8,128)(2,1)} async-done(((bf16[1,256,256]{2,1,0:T(8,128)(2,1)}), bf16[1,2048,256]{2,1,0:T(8,128)(2,1)}) %all-gather.61.cloned.1.call-update) | async-done | bytes 1048592 | tf_op jit(solution)/shard_map/all_gather | solution.py:10
  634.9 4.8 convolution_convert_fusion.1
  639.8 36.3 %all-gather.59.cloned.1.call-done = bf16[1,2048,256]{2,1,0:T(8,128)(2,1)} async-done(((bf16[1,256,256]{2,1,0:T(8,128)(2,1)}), bf16[1,2048,256]{2,1,0:T(8,128)(2,1)}) %all-gather.59.cloned.1.call-update) | async-done | bytes 1048592 | tf_op jit(solution)/shard_map/all_gather | solution.py:10
  676.0 4.9 convolution_convert_fusion.2
  681.1 2.3 collective-permute-start.2
  683.4 1.4 collective-permute-done.2
  684.8 1.5 fusion.14
  686.3 30.8 %all-gather.65.cloned.1.call-done = bf16[1,1024,512]{2,1,0:T(8,128)(2,1)} async-done(((bf16[1,128,512]{2,1,0:T(8,128)(2,1)}), bf16[1,1024,512]{2,1,0:T(8,128)(2,1)}) %all-gather.65.cloned.1.call-update) | async-done | bytes 1048592 | tf_op jit(solution)/shard_map/all_gather | solution.py:10
  717.2 28.8 %all-gather.41.cloned.1.call-done = bf16[6,256,1024]{2,1,0:T(8,128)(2,1)} async-done(((bf16[6,256,256]{2,1,0:T(8,128)(2,1)}), bf16[6,256,1024]{2,1,0:T(8,128)(2,1)}) %all-gather.41.cloned.1.call-update) | async-done | bytes 3145744 | tf_op jit(solution)/shard_map/all_gather | solution.py:90
  745.9 5.6 fusion.30
  (66 shorter events, 9.3 us)
Async XLA Ops:
  6.5 1.0 copy-start.3
  6.5 1.8 copy-start.4
  6.5 2.7 copy-start.5
  6.5 51.4 %all-gather.31.cloned.1.call-start = ((), (), s32[]{:S(2)}) async-start(), calls=%async_computation | async-start | bytes 7864320 | tf_op jit(solution)/shard_map/all_gather | solution.py:70
  7.3 2.8 copy-start.6
  7.3 93.4 %all-gather.47.cloned.1.call-start = ((), (), s32[]{:S(2)}) async-start(), calls=%async_computation.8 | async-start | bytes 1179648 | tf_op jit(solution)/shard_map/all_gather | solution.py:10
  8.3 2.6 copy-start.7
  8.3 133.7 %all-gather.45.cloned.1.call-start = ((), (), s32[]{:S(2)}) async-start(), calls=%async_computation.7 | async-start | bytes 1179648 | tf_op jit(solution)/shard_map/all_gather | solution.py:10
  9.1 173.9 %all-gather.43.cloned.1.call-start = ((), (), s32[]{:S(2)}) async-start(), calls=%async_computation.6 | async-start | bytes 1179648 | tf_op jit(solution)/shard_map/all_gather | solution.py:10
  10.0 214.2 %all-gather.49.cloned.1.call-start = ((), (), s32[]{:S(2)}) async-start(), calls=%async_computation.9 | async-start | bytes 1179648 | tf_op jit(solution)/shard_map/all_gather | solution.py:10
  10.8 242.1 %all-gather.33.cloned.1.call-start = ((), (), s32[]{:S(2)}) async-start(), calls=%async_computation.1 | async-start | bytes 3932160 | tf_op jit(solution)/shard_map/all_gather | solution.py:90
  57.9 4.6 copy-start
  187.9 2.5 copy-start.8
  188.1 3.7 collective-permute-start
  193.3 111.2 %all-gather.35.cloned.1.call-start = ((), (), s32[]{:S(2)}) async-start(), calls=%async_computation.2 | async-start | bytes 7864320 | tf_op jit(solution)/shard_map/all_gather | solution.py:70
  258.1 89.1 %all-gather.55.cloned.1.call-start = ((), (), s32[]{:S(2)}) async-start(), calls=%async_computation.12 | async-start | bytes 1179648 | tf_op jit(solution)/shard_map/all_gather | solution.py:10
  258.8 129.7 %all-gather.53.cloned.1.call-start = ((), (), s32[]{:S(2)}) async-start(), calls=%async_computation.11 | async-start | bytes 1179648 | tf_op jit(solution)/shard_map/all_gather | solution.py:10
  259.6 170.0 %all-gather.51.cloned.1.call-start = ((), (), s32[]{:S(2)}) async-start(), calls=%async_computation.10 | async-start | bytes 1179648 | tf_op jit(solution)/shard_map/all_gather | solution.py:10
  260.2 210.7 %all-gather.57.cloned.1.call-start = ((), (), s32[]{:S(2)}) async-start(), calls=%async_computation.13 | async-start | bytes 1179648 | tf_op jit(solution)/shard_map/all_gather | solution.py:10
  260.9 238.8 %all-gather.37.cloned.1.call-start = ((), (), s32[]{:S(2)}) async-start(), calls=%async_computation.3 | async-start | bytes 3932160 | tf_op jit(solution)/shard_map/all_gather | solution.py:90
  304.5 4.6 copy-start.2
  434.7 3.7 collective-permute-start.1
  439.9 111.3 %all-gather.39.cloned.1.call-start = ((), (), s32[]{:S(2)}) async-start(), calls=%async_computation.4 | async-start | bytes 7864320 | tf_op jit(solution)/shard_map/all_gather | solution.py:70
  504.8 89.0 %all-gather.63.cloned.1.call-start = ((), (), s32[]{:S(2)}) async-start(), calls=%async_computation.16 | async-start | bytes 1179648 | tf_op jit(solution)/shard_map/all_gather | solution.py:10
  505.4 129.5 %all-gather.61.cloned.1.call-start = ((), (), s32[]{:S(2)}) async-start(), calls=%async_computation.15 | async-start | bytes 1179648 | tf_op jit(solution)/shard_map/all_gather | solution.py:10
  506.0 170.1 %all-gather.59.cloned.1.call-start = ((), (), s32[]{:S(2)}) async-start(), calls=%async_computation.14 | async-start | bytes 1179648 | tf_op jit(solution)/shard_map/all_gather | solution.py:10
  506.5 210.6 %all-gather.65.cloned.1.call-start = ((), (), s32[]{:S(2)}) async-start(), calls=%async_computation.17 | async-start | bytes 1179648 | tf_op jit(solution)/shard_map/all_gather | solution.py:10
  507.1 238.8 %all-gather.41.cloned.1.call-start = ((), (), s32[]{:S(2)}) async-start(), calls=%async_computation.5 | async-start | bytes 3932160 | tf_op jit(solution)/shard_map/all_gather | solution.py:90
  551.2 4.6 copy-start.1
  681.1 3.7 collective-permute-start.2
Sparse Core Ops, SparseCore 0:
  8.9 48.9 all-gather.30
  60.1 40.5 all-gather.46
  102.8 39.0 all-gather.44
  143.9 39.0 all-gather.42
  185.0 39.0 all-gather.48
  225.6 27.3 all-gather.32
  258.2 46.2 all-gather.34
  306.6 40.5 all-gather.54
  349.4 39.0 all-gather.52
  390.5 39.0 all-gather.50
  431.8 39.0 all-gather.56
  472.3 27.3 all-gather.36
  504.9 46.2 all-gather.38
  553.2 40.5 all-gather.62
  595.8 39.0 all-gather.60
  636.9 39.0 all-gather.58
  678.0 39.0 all-gather.64
  718.6 27.3 all-gather.40
where the time goes:
time: 759 us; the launch traced here: 758 us
  waiting for transfers between devices  642 us (85%)
  matrix products  59.6 us (8%)
  other arithmetic  30.2 us (4%)
  between operations  13.9 us (2%)
  starting transfers between devices  7.92 us (1%)
    all_gather x12, waiting for transfers between devices, taken_in(): lax.all_gather(part, axis, axis=dim, tiled=True)  412 us
    all_gather x3, waiting for transfers between devices, local(): whole = lax.all_gather(current, 'tp', axis=2, tiled=True)  134 us
    all_gather x3, waiting for transfers between devices, local(): full_mix = lax.all_gather(mixer, 'tp', axis=2, tiled=True)  86.3 us
    dot_general x9, matrix products, add_rows(): jnp.dot(columns, piece, preferred_element_type=jnp.float32)  43.8 us
    dot_general x3, matrix products, add_rows(): return total + jnp.dot(columns, piece, preferred_element_type=jnp.float32)  15.9 us
  transfers between devices with their start and end apart: 21, of which 21 were waited for; matrix products, arithmetic and copies ran while one was open for 10% of the time, Pallas kernels for 0%

commit v1 on v0

v1 whole, which is shorter than its diff:
```python
import functools

import jax
import jax.numpy as jnp
from jax import lax
from jax.experimental import pallas as pl
from jax.experimental.pallas import tpu as pltpu
from jax.sharding import PartitionSpec as P

epsilon = 1e-06


def gather_kernel(plans, *refs):
    count = len(plans)
    shards, wholes, scratch = refs[:count], refs[count : 2 * count], refs[2 * count :]
    jobs = []
    for i, (axis, size, pair, dim) in enumerate(plans):
        me = lax.axis_index(axis)
        jobs.append((axis, size // pair, pair, dim, me // pair, me % pair, shards[i], wholes[i]) + tuple(scratch[6 * i : 6 * i + 6]))

    barrier = pltpu.get_barrier_semaphore()
    expected = jnp.int32(0)
    for axis, length, pair, _, spot, side, *_ in jobs:
        for step in (-1, 1):
            there = jnp.logical_and(spot + step >= 0, spot + step < length)
            expected = expected + there.astype(jnp.int32)

            @pl.when(there)
            def _(axis=axis, target=(spot + step) * pair + side):
                pl.semaphore_signal(barrier, inc=1, device_id={axis: target})

        if pair == 2:
            expected = expected + 1
            pl.semaphore_signal(barrier, inc=1, device_id={axis: spot * pair + 1 - side})
    pl.semaphore_wait(barrier, expected)

    def place(job, owner_spot, owner_side):
        pair, dim, shard, whole = job[2], job[3], job[6], job[7]
        extent = shard.shape[dim]
        start = pl.multiple_of((owner_spot * pair + owner_side) * extent, extent)
        return whole.at[pl.ds(start, extent), :] if dim == 0 else whole.at[:, pl.ds(start, extent)]

    def remote(job, kind, owner, own=False):
        axis, _, pair, _, spot, side, shard, _, line_recv, pair_recv, right, left, across, _ = job
        slot = place(job, owner, side)
        send, recv, target = {
            "right": (right, line_recv, (spot + 1) * pair + side),
            "left": (left, line_recv, (spot - 1) * pair + side),
            "across": (across, pair_recv, spot * pair + 1 - side),
        }[kind]
        return pltpu.make_async_remote_copy(
            src_ref=shard if own else slot,
            dst_ref=slot,
            send_sem=send.at[owner],
            recv_sem=recv.at[owner],
            device_id={axis: target},
        )

    def arrived(job, kind, owner):
        axis, _, pair, _, spot, side, _, _, line_recv, pair_recv, right, _, across, _ = job
        slot = place(job, owner, side if kind == "line" else 1 - side)
        recv = line_recv if kind == "line" else pair_recv
        pltpu.make_async_remote_copy(
            src_ref=slot,
            dst_ref=slot,
            send_sem=across.at[owner],
            recv_sem=recv.at[owner],
            device_id={axis: spot * pair + side},
        ).wait_recv()

    def spread(job, owner, go_right, go_left, own=False):
        spot, length, pair = job[4], job[1], job[2]
        if go_right:
            @pl.when(spot < length - 1)
            def _():
                remote(job, "right", owner, own).start()

        if go_left:
            @pl.when(spot > 0)
            def _():
                remote(job, "left", owner, own).start()

        if pair == 2:
            remote(job, "across", owner, own).start()

    for job in jobs:
        spread(job, job[4], True, True, own=True)
    for job in jobs:
        pltpu.make_async_copy(job[6], place(job, job[4], job[5]), job[13]).start()

    for job in jobs:
        spot, length = job[4], job[1]
        for distance in range(1, length):

            @pl.when(spot >= distance)
            def _(job=job, owner=spot - distance):
                arrived(job, "line", owner)
                spread(job, owner, True, False)

            @pl.when(spot + distance < length)
            def _(job=job, owner=spot + distance):
                arrived(job, "line", owner)
                spread(job, owner, False, True)

    for job in jobs:
        spot, length, pair = job[4], job[1], job[2]
        pltpu.make_async_copy(job[6], place(job, job[4], job[5]), job[13]).wait()
        for owner in range(length):
            if pair == 2:
                arrived(job, "across", owner)
                remote(job, "across", owner).wait_send()

            @pl.when(jnp.logical_and(spot >= owner, spot < length - 1))
            def _(job=job, owner=owner):
                remote(job, "right", owner).wait_send()

            @pl.when(jnp.logical_and(spot <= owner, spot > 0))
            def _(job=job, owner=owner):
                remote(job, "left", owner).wait_send()


def gather_all(parts, number):
    plans, shapes, scratch, sent = [], [], [], 0
    for array, axis, dim in parts:
        size = lax.axis_size(axis)
        pair = 2 if size % 2 == 0 else 1
        plans.append((axis, size, pair, dim))
        shape = list(array.shape)
        shape[dim] *= size
        shapes.append(jax.ShapeDtypeStruct(tuple(shape), array.dtype))
        sent += array.size * array.dtype.itemsize * size
        scratch += [pltpu.SemaphoreType.DMA((size // pair,))] * 5 + [pltpu.SemaphoreType.DMA]
    return pl.pallas_call(
        functools.partial(gather_kernel, tuple(plans)),
        out_shape=tuple(shapes),
        in_specs=[pl.BlockSpec(memory_space=pltpu.VMEM)] * len(parts),
        out_specs=tuple([pl.BlockSpec(memory_space=pl.ANY)] * len(parts)),
        scratch_shapes=scratch,
        cost_estimate=pl.CostEstimate(flops=0, bytes_accessed=10 * sent, transcendentals=0),
        compiler_params=pltpu.CompilerParams(collective_id=number, has_side_effects=True),
    )(*[array for array, _, _ in parts])


def from_behind(block, axis, distance):
    devices = range(lax.axis_size(axis))
    route = [(i - distance, i) for i in devices if i - distance in devices]
    return lax.ppermute(block, axis, route)


def normalize(values_in, gain_row):
    values = values_in.astype(jnp.float32)
    scale = lax.rsqrt(jnp.mean(values * values, axis=-1, keepdims=True) + epsilon)
    return (values * scale * gain_row.astype(jnp.float32)).astype(jnp.bfloat16)


def convolve(extended, taps):
    width = taps.shape[0]
    out_rows = extended.shape[1] - (width - 1)
    total = jnp.zeros((extended.shape[0], out_rows, extended.shape[2]), jnp.float32)
    for offset in range(width):
        total = total + taps[offset].astype(jnp.float32) * extended[:, offset : offset + out_rows]
    return total


def local(tokens, norm_gains, weight_outer, weight_inner, weight_value, conv_taps, weight_output):
    layers = conv_taps.shape[0]
    history = conv_taps.shape[1] - 1
    sequences, rows, width = tokens.shape
    channels = weight_outer.shape[2]
    weight_in = jnp.concatenate([weight_outer, weight_inner, weight_value], axis=2)
    current = tokens.reshape(sequences * rows, width)
    result = None
    for layer in range(layers):
        joined, whole = gather_all([(weight_in[layer], "sp", 0), (current, "tp", 1)], 2 * layer)
        normed = normalize(whole, norm_gains[layer])
        gates = jnp.dot(normed, joined, preferred_element_type=jnp.float32).astype(jnp.bfloat16)
        outer, inner, value = (
            gates[:, i * channels : (i + 1) * channels].reshape(sequences, rows, channels)
            for i in range(3)
        )
        gated = inner.astype(jnp.float32) * value.astype(jnp.float32)
        earlier = from_behind(gated[:, rows - history :], "sp", 1)
        extended = jnp.concatenate([earlier, gated], axis=1)
        conved = convolve(extended, conv_taps[layer])
        mixer = (outer.astype(jnp.float32) * conved).astype(jnp.bfloat16)
        flat_mixer = mixer.reshape(sequences * rows, channels)
        weight_down, full_mix = gather_all(
            [(weight_output[layer], "sp", 0), (flat_mixer, "tp", 1)], 2 * layer + 1
        )
        result = jnp.dot(full_mix, weight_down, preferred_element_type=jnp.float32)
        current = result.astype(jnp.bfloat16)
    return result.reshape(sequences, rows, width)


def solution(mesh):
    placed = (
        P(None, "sp", "tp"),
        P(),
        P(None, "sp", "tp"),
        P(None, "sp", "tp"),
        P(None, "sp", "tp"),
        P(None, None, "tp"),
        P(None, "sp", "tp"),
    )
    return jax.shard_map(
        local, mesh=mesh, in_specs=placed, out_specs=P(None, "sp", "tp"), check_vma=False
    )
```

time: 759 us -> 278 us (0.37)
  waiting for transfers between devices: 642 us -> 3.19 us
  Pallas kernels: 0 us -> 204 us
  matrix products: 59.6 us -> 38.4 us
  between operations: 13.9 us -> 0.28 us
  other arithmetic: 30.2 us -> 17.7 us
    all_gather x18 -> x0, waiting for transfers between devices: 633 us -> none  [the longest x12 412 us: taken_in(): lax.all_gather(part, axis, axis=dim, tiled=True)]
    pallas_call x0 -> x6, Pallas kernels: none -> 204 us  [gather_all(): pl.pallas_call(functools.partial(gather_kernel, tuple(plans)), out_shape=...]
    dot_general x12 -> x6, matrix products: 59.6 us -> 38.4 us  [the longest x3 22.6 us: local(): jnp.dot(normed, joined, preferred_element_type=jnp.float32)]
    convert_element_type x6 -> x3, other arithmetic: 16.9 us -> 4.47 us  [local(): mixer = (outer.astype(jnp.float32) * conved).astype(jnp.bfloat16)]
  transfers between devices with their start and end apart: 21 -> 3, of which waited for: 21 -> 3; matrix products, arithmetic and copies ran while one was open for 10% -> 0% of each run, Pallas kernels for 0% -> 0%
where the time goes in v1:
time: 278 us
  Pallas kernels  204 us (73%)
  matrix products  38.4 us (14%)
  other arithmetic  17.7 us (6%)
  starting transfers between devices  9.22 us (3%)
  local copies, waits for them, and re-layouts  5.15 us (2%)
  waiting for transfers between devices  3.19 us (1%)
    pallas_call x6, Pallas kernels, gather_all(): pl.pallas_call(functools.partial(gather_kernel, tuple(plans)), out_shape=...  204 us
    dot_general x3, matrix products, local(): jnp.dot(normed, joined, preferred_element_type=jnp.float32)  22.6 us
    dot_general x3, matrix products, local(): result = jnp.dot(full_mix, weight_down, preferred_element_type=jnp.float32)  15.9 us
    reduce_sum x3, other arithmetic, normalize(): jnp.mean(values * values, axis=-1, keepdims=True) + epsilon  12.7 us
    ppermute x3, starting transfers between devices, from_behind(): return lax.ppermute(block, axis, route)  9.22 us
  transfers between devices with their start and end apart: 3, of which 3 were waited for; matrix products, arithmetic and copies ran while one was open for 0% of the time, Pallas kernels for 0%

profile of v1, /device:TPU:0, one launch (start us, length us, event | category | flops | bytes accessed | tf_op | source)
XLA Modules:
  0.0 277.8 jit_solution(4290305453813334820)
XLA Ops:
  0.0 0.0 copy-start.3
  0.0 1.1 constant_dynamic-update-slice_fusion.2
  1.1 1.0 constant_dynamic-update-slice_fusion.1
  2.1 0.0 copy-done.3
  2.2 1.0 slice_bitcast_fusion
  3.2 0.0 copy-start.5
  3.2 44.0 %shard_map.73 = (bf16[2048,768]{1,0:T(8,128)(2,1)}, bf16[1536,2048]{1,0:T(8,128)(2,1)}) custom-call(bf16[256,768]{1,0:T(8,128)(2,1)} %get-tuple-element.29.refs_0_, bf16[1536,512]{1,0:T(8,128)(2,1)} %bitcast.59), custom_call_target="tpu_custom_call" | custom-call | bytes 94371840 | tf_op jit(solution)/shard_map/pallas_call | solution.py:133
  47.2 0.0 copy-start
  47.2 4.2 %fusion = f32[1536]{0:T(1024)S(1)} fusion(bf16[1536,2048]{1,0:T(8,128)(2,1)} %get-tuple-element.17), kind=kLoop, calls=%fused_computation.6 | loop fusion | flops 9435648 | bytes 6297600 | tf_op jit(solution)/shard_map/reduce_sum | solution.py:152
  51.4 0.0 copy-done.5
  51.5 0.3 copy-done
  51.8 7.5 %fusion.21 = bf16[1536,768]{1,0:T(8,128)(2,1)S(1)} fusion(bf16[2048,768]{1,0:T(8,128)(2,1)} %get-tuple-element.18, bf16[1536,2048]{1,0:T(8,128)(2,1)S(1)} %copy-done, f32[2048]{0:T(1024)S(1)} %bitcast.62, f32[1536]{0:T(1024)S(1)} %add_rsqrt_fusion.2), kind=kOutput, calls=%fused_computation.24 | convolution fusion | flops 4845600768 | bytes 11810816 | tf_op jit(solution)/shard_map/dot_general | solution.py:176
  59.3 0.0 copy-start.4
  59.3 0.0 copy-start.6
  59.3 0.2 convert_multiply_fusion.8
  59.5 3.4 %collective-permute-start = (f32[6,2,256]{2,1,0:T(2,128)S(1)}, f32[6,2,256]{2,1,0:T(2,128)S(1)}, u32[]{:S(2)}, u32[]{:S(2)}) collective-permute-start(f32[6,2,256]{2,1,0:T(2,128)S(1)} %slice.171), channel_id=1, source_target_pairs={{0,4},{4,8},{8,12},{12,16},{16,20},{20,24},{24,28},{1,5},{5,9},{9,... | collective-permute-start | bytes 36872 | tf_op jit(solution)/shard_map/ppermute | solution.py:147
  63.0 0.0 copy-done.4
  63.0 0.8 slice_bitcast_fusion.3
  63.7 0.0 copy-done.6
  63.7 0.1 slice.168
  63.8 0.5 collective-permute-done
  64.3 1.5 fusion.47
  65.8 24.3 %shard_map.74 = (bf16[1024,512]{1,0:T(8,128)(2,1)}, bf16[1536,1024]{1,0:T(8,128)(2,1)}) custom-call(bf16[128,512]{1,0:T(8,128)(2,1)} %get-tuple-element.32.refs_0_, bf16[1536,256]{1,0:T(8,128)(2,1)} %bitcast.57), custom_call_target="tpu_custom_call" | custom-call | bytes 41943040 | tf_op jit(solution)/shard_map/pallas_call | solution.py:133
  90.1 5.1 %convolution_convert_fusion.1.refs_1_ = bf16[1536,512]{1,0:T(8,128)(2,1)} fusion(bf16[1536,1024]{1,0:T(8,128)(2,1)} %get-tuple-element.19, bf16[1024,512]{1,0:T(8,128)(2,1)} %get-tuple-element.20), kind=kOutput, calls=%fused_computation.28 | convolution fusion | flops 1611399168 | bytes 5767168 | tf_op jit(solution)/shard_map/dot_general | solution.py:190
  95.3 43.6 %shard_map.75 = (bf16[2048,768]{1,0:T(8,128)(2,1)}, bf16[1536,2048]{1,0:T(8,128)(2,1)}) custom-call(bf16[256,768]{1,0:T(8,128)(2,1)} %get-tuple-element.30.refs_0_, bf16[1536,512]{1,0:T(8,128)(2,1)} %convolution_convert_fusion.1.refs_1_), custom_call_target="tpu_custom_call" | custom-call | bytes 94371840 | tf_op jit(solution)/shard_map/pallas_call | solution.py:133
  138.9 0.0 copy-start.2
  138.9 4.2 %fusion.3 = f32[1536]{0:T(1024)S(1)} fusion(bf16[1536,2048]{1,0:T(8,128)(2,1)} %get-tuple-element.21), kind=kLoop, calls=%fused_computation.9 | loop fusion | flops 9435648 | bytes 6297600 | tf_op jit(solution)/shard_map/reduce_sum | solution.py:152
  143.1 0.3 copy-done.2
  143.5 7.5 %fusion.24 = bf16[1536,768]{1,0:T(8,128)(2,1)S(1)} fusion(bf16[2048,768]{1,0:T(8,128)(2,1)} %get-tuple-element.22, bf16[1536,2048]{1,0:T(8,128)(2,1)S(1)} %copy-done.2, f32[2048]{0:T(1024)S(1)} %bitcast.61, f32[1536]{0:T(1024)S(1)} %add_rsqrt_fusion.1), kind=kOutput, calls=%fused_computation.25 | convolution fusion | flops 4845600768 | bytes 11810816 | tf_op jit(solution)/shard_map/dot_general | solution.py:176
  151.0 0.2 convert_multiply_fusion.7
  151.2 3.4 %collective-permute-start.1 = (f32[6,2,256]{2,1,0:T(2,128)S(1)}, f32[6,2,256]{2,1,0:T(2,128)S(1)}, u32[]{:S(2)}, u32[]{:S(2)}) collective-permute-start(f32[6,2,256]{2,1,0:T(2,128)S(1)} %slice.177), channel_id=1, source_target_pairs={{0,4},{4,8},{8,12},{12,16},{16,20},{20,24},{24,28},{1,5},{5,9},{9,... | collective-permute-start | bytes 36872 | tf_op jit(solution)/shard_map/ppermute | solution.py:147
  154.6 0.1 slice.174
  154.6 1.3 collective-permute-done.1
  155.9 1.5 fusion.41
  157.4 23.7 %shard_map.76 = (bf16[1024,512]{1,0:T(8,128)(2,1)}, bf16[1536,1024]{1,0:T(8,128)(2,1)}) custom-call(bf16[128,512]{1,0:T(8,128)(2,1)} %get-tuple-element.34.refs_0_, bf16[1536,256]{1,0:T(8,128)(2,1)} %bitcast.58), custom_call_target="tpu_custom_call" | custom-call | bytes 41943040 | tf_op jit(solution)/shard_map/pallas_call | solution.py:133
  181.2 5.1 %convolution_convert_fusion.refs_1_ = bf16[1536,512]{1,0:T(8,128)(2,1)} fusion(bf16[1536,1024]{1,0:T(8,128)(2,1)} %get-tuple-element.23, bf16[1024,512]{1,0:T(8,128)(2,1)} %get-tuple-element.24), kind=kOutput, calls=%fused_computation.27 | convolution fusion | flops 1611399168 | bytes 5767168 | tf_op jit(solution)/shard_map/dot_general | solution.py:190
  186.3 43.5 %shard_map.77 = (bf16[2048,768]{1,0:T(8,128)(2,1)}, bf16[1536,2048]{1,0:T(8,128)(2,1)}) custom-call(bf16[256,768]{1,0:T(8,128)(2,1)} %get-tuple-element.31.refs_0_, bf16[1536,512]{1,0:T(8,128)(2,1)} %convolution_convert_fusion.refs_1_), custom_call_target="tpu_custom_call" | custom-call | bytes 94371840 | tf_op jit(solution)/shard_map/pallas_call | solution.py:133
  229.8 0.0 copy-start.1
  229.8 4.2 %fusion.6 = f32[1536]{0:T(1024)S(1)} fusion(bf16[1536,2048]{1,0:T(8,128)(2,1)} %get-tuple-element.25), kind=kLoop, calls=%fused_computation.12 | loop fusion | flops 9435648 | bytes 6297600 | tf_op jit(solution)/shard_map/reduce_sum | solution.py:152
  234.1 0.3 copy-done.1
  234.4 7.5 %fusion.27 = bf16[1536,768]{1,0:T(8,128)(2,1)S(1)} fusion(bf16[2048,768]{1,0:T(8,128)(2,1)} %get-tuple-element.26, bf16[1536,2048]{1,0:T(8,128)(2,1)S(1)} %copy-done.1, f32[2048]{0:T(1024)S(1)} %bitcast.60, f32[1536]{0:T(1024)S(1)} %add_rsqrt_fusion), kind=kOutput, calls=%fused_computation.26 | convolution fusion | flops 4845600768 | bytes 11810816 | tf_op jit(solution)/shard_map/dot_general | solution.py:176
  242.0 0.2 convert_multiply_fusion.6
  242.2 2.4 collective-permute-start.2
  244.6 0.1 slice.180
  244.6 1.3 collective-permute-done.2
  246.0 1.5 fusion.35
  247.5 24.7 %shard_map.78 = (bf16[1024,512]{1,0:T(8,128)(2,1)}, bf16[1536,1024]{1,0:T(8,128)(2,1)}) custom-call(bf16[128,512]{1,0:T(8,128)(2,1)} %get-tuple-element.33.refs_0_, bf16[1536,256]{1,0:T(8,128)(2,1)} %bitcast.56), custom_call_target="tpu_custom_call" | custom-call | bytes 41943040 | tf_op jit(solution)/shard_map/pallas_call | solution.py:133
  272.2 5.6 %fusion.52 = f32[1536,512]{1,0:T(8,128)} fusion(bf16[1536,1024]{1,0:T(8,128)(2,1)} %get-tuple-element.27, bf16[1024,512]{1,0:T(8,128)(2,1)} %get-tuple-element.28), kind=kOutput, calls=%fused_computation.84 | convolution fusion | flops 1610612736 | bytes 7340032 | tf_op jit(solution)/shard_map/dot_general | solution.py:190
  (9 shorter events, 0.1 us)
Async XLA Ops:
  0.0 2.1 copy-start.3
  3.2 48.3 %copy-start.5 = (f32[3,2048]{1,0:T(4,128)S(1)}, f32[3,2048]{1,0:T(4,128)}, u32[]{:S(2)}) copy-start(f32[3,2048]{1,0:T(4,128)} %param.8) | copy-start | bytes 73732
  47.2 4.6 %copy-start = (bf16[1536,2048]{1,0:T(8,128)(2,1)S(1)}, bf16[1536,2048]{1,0:T(8,128)(2,1)}, u32[]{:S(2)}) copy-start(bf16[1536,2048]{1,0:T(8,128)(2,1)} %get-tuple-element.17) | copy-start | bytes 18874372
  59.3 3.6 %copy-start.4 = (bf16[3,128,512]{2,1,0:T(8,128)(2,1)S(1)}, bf16[3,128,512]{2,1,0:T(8,128)(2,1)}, u32[]{:S(2)}) copy-start(bf16[3,128,512]{2,1,0:T(8,128)(2,1)} %param.13) | copy-start | bytes 1179652
  59.3 4.4 %copy-start.6 = (bf16[3,3,256]{2,1,0:T(4,128)(2,1)S(1)}, bf16[3,3,256]{2,1,0:T(4,128)(2,1)}, u32[]{:S(2)}) copy-start(bf16[3,3,256]{2,1,0:T(4,128)(2,1)} %param.12) | copy-start | bytes 13828
  59.5 4.8 %collective-permute-start = (f32[6,2,256]{2,1,0:T(2,128)S(1)}, f32[6,2,256]{2,1,0:T(2,128)S(1)}, u32[]{:S(2)}, u32[]{:S(2)}) collective-permute-start(f32[6,2,256]{2,1,0:T(2,128)S(1)} %slice.171), channel_id=1, source_target_pairs={{0,4},{4,8},{8,12},{12,16},{16,20},{20,24},{24,28},{1,5},{5,9},{9,... | collective-permute-start | bytes 36872 | tf_op jit(solution)/shard_map/ppermute | solution.py:147
  138.9 4.6 %copy-start.2 = (bf16[1536,2048]{1,0:T(8,128)(2,1)S(1)}, bf16[1536,2048]{1,0:T(8,128)(2,1)}, u32[]{:S(2)}) copy-start(bf16[1536,2048]{1,0:T(8,128)(2,1)} %get-tuple-element.21) | copy-start | bytes 18874372
  151.2 4.8 %collective-permute-start.1 = (f32[6,2,256]{2,1,0:T(2,128)S(1)}, f32[6,2,256]{2,1,0:T(2,128)S(1)}, u32[]{:S(2)}, u32[]{:S(2)}) collective-permute-start(f32[6,2,256]{2,1,0:T(2,128)S(1)} %slice.177), channel_id=1, source_target_pairs={{0,4},{4,8},{8,12},{12,16},{16,20},{20,24},{24,28},{1,5},{5,9},{9,... | collective-permute-start | bytes 36872 | tf_op jit(solution)/shard_map/ppermute | solution.py:147
  229.8 4.6 %copy-start.1 = (bf16[1536,2048]{1,0:T(8,128)(2,1)S(1)}, bf16[1536,2048]{1,0:T(8,128)(2,1)}, u32[]{:S(2)}) copy-start(bf16[1536,2048]{1,0:T(8,128)(2,1)} %get-tuple-element.25) | copy-start | bytes 18874372
  242.2 3.8 %collective-permute-start.2 = (f32[6,2,256]{2,1,0:T(2,128)S(1)}, f32[6,2,256]{2,1,0:T(2,128)S(1)}, u32[]{:S(2)}, u32[]{:S(2)}) collective-permute-start(f32[6,2,256]{2,1,0:T(2,128)S(1)} %slice.183), channel_id=1, source_target_pairs={{0,4},{4,8},{8,12},{12,16},{16,20},{20,24},{24,28},{1,5},{5,9},{9,... | collective-permute-start | bytes 36872 | tf_op jit(solution)/shard_map/ppermute | solution.py:147

commit v2 on v0

v2 whole, which is shorter than its diff:
```python
import functools

import jax
import jax.numpy as jnp
from jax import lax
from jax.experimental import pallas as pl
from jax.experimental.pallas import tpu as pltpu
from jax.sharding import PartitionSpec as P

epsilon = 1e-06


class Gather:
    def __init__(self, axis, size, dim, shard, whole, sems):
        self.axis, self.dim, self.shard, self.whole = axis, dim, shard, whole
        self.pair = 2 if size % 2 == 0 else 1
        self.length = size // self.pair
        me = lax.axis_index(axis)
        self.spot, self.side = me // self.pair, me % self.pair
        self.line_recv, self.pair_recv, self.right, self.left, self.across, self.own = sems

    def place(self, spot, side):
        extent = self.shard.shape[self.dim]
        start = pl.multiple_of((spot * self.pair + side) * extent, extent)
        cut = pl.ds(start, extent)
        return self.whole.at[cut, :] if self.dim == 0 else self.whole.at[:, cut]

    def remote(self, kind, owner, own=False):
        slot = self.place(owner, self.side)
        send, recv, target = {
            "right": (self.right, self.line_recv, (self.spot + 1) * self.pair + self.side),
            "left": (self.left, self.line_recv, (self.spot - 1) * self.pair + self.side),
            "across": (self.across, self.pair_recv, self.spot * self.pair + 1 - self.side),
        }[kind]
        return pltpu.make_async_remote_copy(
            src_ref=self.shard if own else slot,
            dst_ref=slot,
            send_sem=send.at[owner],
            recv_sem=recv.at[owner],
            device_id={self.axis: target},
        )

    def arrived(self, side, recv, owner):
        slot = self.place(owner, side)
        pltpu.make_async_remote_copy(
            src_ref=slot,
            dst_ref=slot,
            send_sem=self.across.at[owner],
            recv_sem=recv.at[owner],
            device_id={self.axis: self.spot * self.pair + self.side},
        ).wait_recv()

    def spread(self, owner, go_right, go_left, own=False):
        if go_right:
            @pl.when(self.spot < self.length - 1)
            def _():
                self.remote("right", owner, own).start()

        if go_left:
            @pl.when(self.spot > 0)
            def _():
                self.remote("left", owner, own).start()

        if self.pair == 2:
            self.remote("across", owner, own).start()

    def local(self):
        return pltpu.make_async_copy(self.shard, self.place(self.spot, self.side), self.own)

    def start(self):
        self.spread(self.spot, True, True, own=True)
        self.local().start()

    def step(self, distance):
        @pl.when(self.spot >= distance)
        def _():
            self.arrived(self.side, self.line_recv, self.spot - distance)
            self.spread(self.spot - distance, True, False)

        @pl.when(self.spot + distance < self.length)
        def _():
            self.arrived(self.side, self.line_recv, self.spot + distance)
            self.spread(self.spot + distance, False, True)

    def steps(self):
        return [functools.partial(self.step, distance) for distance in range(1, self.length)]

    def complete(self):
        self.local().wait()
        if self.pair == 2:
            for owner in range(self.length):
                self.arrived(1 - self.side, self.pair_recv, owner)

    def drain(self):
        for owner in range(self.length):
            if self.pair == 2:
                self.remote("across", owner).wait_send()

            @pl.when(jnp.logical_and(self.spot >= owner, self.spot < self.length - 1))
            def _(owner=owner):
                self.remote("right", owner).wait_send()

            @pl.when(jnp.logical_and(self.spot <= owner, self.spot > 0))
            def _(owner=owner):
                self.remote("left", owner).wait_send()


def greet(gathers):
    barrier = pltpu.get_barrier_semaphore()
    expected = jnp.int32(0)
    for g in gathers:
        for step in (-1, 1):
            there = jnp.logical_and(g.spot + step >= 0, g.spot + step < g.length)
            expected = expected + there.astype(jnp.int32)

            @pl.when(there)
            def _(g=g, step=step):
                target = (g.spot + step) * g.pair + g.side
                pl.semaphore_signal(barrier, inc=1, device_id={g.axis: target})

        if g.pair == 2:
            expected = expected + 1
            target = g.spot * g.pair + 1 - g.side
            pl.semaphore_signal(barrier, inc=1, device_id={g.axis: target})
    pl.semaphore_wait(barrier, expected)


def alternate(first, second):
    for i in range(max(len(first), len(second))):
        for actions in (first, second):
            if i < len(actions):
                actions[i]()


def sems_of(size, times=1):
    length = size // 2 if size % 2 == 0 else size
    return ([pltpu.SemaphoreType.DMA((length,))] * 5 + [pltpu.SemaphoreType.DMA]) * times


def cut_up(axis, size, pieces, shard, whole, sems):
    rows = shard.shape[0] // pieces
    return [
        Gather(axis, size, 1, shard.at[pl.ds(i * rows, rows)], whole.at[pl.ds(i * rows, rows)], sems[6 * i : 6 * i + 6])
        for i in range(pieces)
    ]


def gather_kernel(sizes, pieces, weight, acts, weight_out, acts_out, *sems):
    weights = Gather("sp", sizes[0], 0, weight, weight_out, sems[:6])
    chunks = cut_up("tp", sizes[1], pieces, acts, acts_out, sems[6:])
    greet([weights, chunks[0]])
    weights.start()
    for chunk in chunks:
        chunk.start()
    alternate([act for chunk in chunks for act in chunk.steps()], weights.steps())
    for each in chunks + [weights]:
        each.complete()
        each.drain()


def boundary_kernel(sizes, pieces, down, weight, mixer, weight_out, acts_out, down_all, mix_all, acts, *sems):
    downs = Gather("sp", sizes[0], 0, down, down_all, sems[:6])
    weights = Gather("sp", sizes[0], 0, weight, weight_out, sems[6:12])
    mixes = cut_up("tp", sizes[1], pieces, mixer, mix_all, sems[12 : 12 + 6 * pieces])
    chunks = cut_up("tp", sizes[1], pieces, acts, acts_out, sems[12 + 6 * pieces :])
    rows = mixer.shape[0] // pieces
    greet([downs, mixes[0]])
    downs.start()
    for mix in mixes:
        mix.start()
    for act in downs.steps():
        act()
    weights.start()
    downs.complete()
    for i in range(pieces):
        for act in mixes[i].steps():
            act()
        mixes[i].complete()
        cut = pl.ds(i * rows, rows)
        acts[cut, :] = jnp.dot(
            mix_all[cut, :], down_all[...], preferred_element_type=jnp.float32
        ).astype(acts.dtype)
        chunks[i].start()
    alternate([act for chunk in chunks for act in chunk.steps()], weights.steps())
    for each in chunks + [weights]:
        each.complete()
    for each in [downs] + mixes + chunks + [weights]:
        each.drain()


def grown(array, dim, size):
    shape = list(array.shape)
    shape[dim] *= size
    return jax.ShapeDtypeStruct(tuple(shape), array.dtype)


def gather_both(weight, acts, pieces, number):
    sizes = lax.axis_size("sp"), lax.axis_size("tp")
    return pl.pallas_call(
        functools.partial(gather_kernel, sizes, pieces),
        out_shape=(grown(weight, 0, sizes[0]), grown(acts, 1, sizes[1])),
        in_specs=[pl.BlockSpec(memory_space=pltpu.VMEM)] * 2,
        out_specs=(pl.BlockSpec(memory_space=pl.ANY),) * 2,
        scratch_shapes=sems_of(sizes[0]) + sems_of(sizes[1], pieces),
        compiler_params=pltpu.CompilerParams(collective_id=number, has_side_effects=True),
    )(weight, acts)


def cross_boundary(down, weight, mixer, pieces, number):
    sizes = lax.axis_size("sp"), lax.axis_size("tp")
    acts = jax.ShapeDtypeStruct((mixer.shape[0], down.shape[1]), mixer.dtype)
    down_all, mix_all = grown(down, 0, sizes[0]), grown(mixer, 1, sizes[1])
    return pl.pallas_call(
        functools.partial(boundary_kernel, sizes, pieces),
        out_shape=(grown(weight, 0, sizes[0]), grown(acts, 1, sizes[1])),
        in_specs=[pl.BlockSpec(memory_space=pltpu.VMEM)] * 3,
        out_specs=(pl.BlockSpec(memory_space=pl.ANY),) * 2,
        scratch_shapes=[pltpu.VMEM(a.shape, a.dtype) for a in (down_all, mix_all, acts)]
        + sems_of(sizes[0], 2)
        + sems_of(sizes[1], 2 * pieces),
        compiler_params=pltpu.CompilerParams(collective_id=number, has_side_effects=True),
    )(down, weight, mixer)


def from_behind(block, axis, distance):
    devices = range(lax.axis_size(axis))
    route = [(i - distance, i) for i in devices if i - distance in devices]
    return lax.ppermute(block, axis, route)


def normalize(values_in, gain_row):
    values = values_in.astype(jnp.float32)
    scale = lax.rsqrt(jnp.mean(values * values, axis=-1, keepdims=True) + epsilon)
    return (values * scale * gain_row.astype(jnp.float32)).astype(jnp.bfloat16)


def convolve(extended, taps):
    width = taps.shape[0]
    out_rows = extended.shape[1] - (width - 1)
    total = jnp.zeros((extended.shape[0], out_rows, extended.shape[2]), jnp.float32)
    for offset in range(width):
        total = total + taps[offset].astype(jnp.float32) * extended[:, offset : offset + out_rows]
    return total


def local(tokens, norm_gains, weight_outer, weight_inner, weight_value, conv_taps, weight_output):
    layers = conv_taps.shape[0]
    history = conv_taps.shape[1] - 1
    sequences, rows, width = tokens.shape
    channels = weight_outer.shape[2]
    weight_in = jnp.concatenate([weight_outer, weight_inner, weight_value], axis=2)
    joined, whole = gather_both(
        weight_in[0], tokens.reshape(sequences * rows, width), sequences, 0
    )
    for layer in range(layers):
        normed = normalize(whole, norm_gains[layer])
        gates = jnp.dot(normed, joined, preferred_element_type=jnp.float32).astype(jnp.bfloat16)
        outer, inner, value = (
            gates[:, i * channels : (i + 1) * channels].reshape(sequences, rows, channels)
            for i in range(3)
        )
        gated = inner.astype(jnp.float32) * value.astype(jnp.float32)
        earlier = from_behind(gated[:, rows - history :], "sp", 1)
        extended = jnp.concatenate([earlier, gated], axis=1)
        conved = convolve(extended, conv_taps[layer])
        mixer = (outer.astype(jnp.float32) * conved).astype(jnp.bfloat16)
        mixer = mixer.reshape(sequences * rows, channels)
        if layer < layers - 1:
            joined, whole = cross_boundary(
                weight_output[layer], weight_in[layer + 1], mixer, sequences, layer + 1
            )
    down, full_mix = gather_both(weight_output[layers - 1], mixer, sequences, layers)
    result = jnp.dot(full_mix, down, preferred_element_type=jnp.float32)
    return result.reshape(sequences, rows, width)


def solution(mesh):
    placed = (
        P(None, "sp", "tp"),
        P(),
        P(None, "sp", "tp"),
        P(None, "sp", "tp"),
        P(None, "sp", "tp"),
        P(None, None, "tp"),
        P(None, "sp", "tp"),
    )
    return jax.shard_map(
        local, mesh=mesh, in_specs=placed, out_specs=P(None, "sp", "tp"), check_vma=False
    )
```

time: 759 us -> 258 us (0.34)
  waiting for transfers between devices: 642 us -> 2.98 us
  Pallas kernels: 0 us -> 195 us
  matrix products: 59.6 us -> 28.2 us
  between operations: 13.9 us -> 0.26 us
  other arithmetic: 30.2 us -> 17.7 us
    all_gather x18 -> x0, waiting for transfers between devices: 633 us -> none  [the longest x12 412 us: taken_in(): lax.all_gather(part, axis, axis=dim, tiled=True)]
    pallas_call x0 -> x4, Pallas kernels: none -> 195 us  [the longest x2 127 us: cross_boundary(): pl.pallas_call(functools.partial(boundary_kernel, sizes, pieces), out_sha...]
    dot_general x12 -> x4, matrix products: 59.6 us -> 28.2 us  [the longest x3 22.5 us: local(): jnp.dot(normed, joined, preferred_element_type=jnp.float32)]
    convert_element_type x6 -> x3, other arithmetic: 16.9 us -> 4.47 us  [local(): mixer = (outer.astype(jnp.float32) * conved).astype(jnp.bfloat16)]
  transfers between devices with their start and end apart: 21 -> 3, of which waited for: 21 -> 3; matrix products, arithmetic and copies ran while one was open for 10% -> 0% of each run, Pallas kernels for 0% -> 0%
where the time goes in v2:
time: 258 us; the launch traced here: 257 us
  Pallas kernels  195 us (76%)
  matrix products  28.2 us (11%)
  other arithmetic  17.7 us (7%)
  starting transfers between devices  8.19 us (3%)
  local copies, waits for them, and re-layouts  5.18 us (2%)
  waiting for transfers between devices  2.98 us (1%)
    pallas_call x2, Pallas kernels, cross_boundary(): pl.pallas_call(functools.partial(boundary_kernel, sizes, pieces), out_sha...  127 us
    pallas_call x2, Pallas kernels, gather_both(): pl.pallas_call(functools.partial(gather_kernel, sizes, pieces), out_shape...  68.3 us
    dot_general x3, matrix products, local(): jnp.dot(normed, joined, preferred_element_type=jnp.float32)  22.5 us
    reduce_sum x3, other arithmetic, normalize(): jnp.mean(values * values, axis=-1, keepdims=True) + epsilon  12.7 us
    ppermute x3, starting transfers between devices, from_behind(): return lax.ppermute(block, axis, route)  8.19 us
    dot_general x1, matrix products, local(): result = jnp.dot(full_mix, down, preferred_element_type=jnp.float32)  5.64 us
  transfers between devices with their start and end apart: 3, of which 3 were waited for; matrix products, arithmetic and copies ran while one was open for 0% of the time, Pallas kernels for 0%

profile of v2, /device:TPU:0, one launch (start us, length us, event | category | flops | bytes accessed | tf_op | source)
XLA Modules:
  0.0 257.2 jit_solution(13105629673627828492)
XLA Ops:
  0.0 0.0 copy-start.3
  0.0 1.1 constant_dynamic-update-slice_fusion.2
  1.1 1.0 constant_dynamic-update-slice_fusion.1
  2.1 0.0 copy-done.3
  2.2 1.0 slice_bitcast_fusion
  3.2 0.0 copy-start.5
  3.2 44.5 %shard_map.73 = (bf16[2048,768]{1,0:T(8,128)(2,1)}, bf16[1536,2048]{1,0:T(8,128)(2,1)}) custom-call(bf16[256,768]{1,0:T(8,128)(2,1)} %get-tuple-element.21.weight, bf16[1536,512]{1,0:T(8,128)(2,1)} %bitcast.55), custom_call_target="tpu_custom_call" | custom-call | tf_op jit(solution)/shard_map/pallas_call | solution.py:199
  47.7 0.0 copy-start
  47.7 4.2 %fusion = f32[1536]{0:T(1024)S(1)} fusion(bf16[1536,2048]{1,0:T(8,128)(2,1)} %get-tuple-element.13), kind=kLoop, calls=%fused_computation.6 | loop fusion | flops 9435648 | bytes 6297600 | tf_op jit(solution)/shard_map/reduce_sum | solution.py:233
  51.9 0.0 copy-done.5
  52.0 0.3 copy-done
  52.3 7.5 %fusion.21 = bf16[1536,768]{1,0:T(8,128)(2,1)S(1)} fusion(bf16[2048,768]{1,0:T(8,128)(2,1)} %get-tuple-element.14, bf16[1536,2048]{1,0:T(8,128)(2,1)S(1)} %copy-done, f32[2048]{0:T(1024)S(1)} %bitcast.58, f32[1536]{0:T(1024)S(1)} %add_rsqrt_fusion.2), kind=kOutput, calls=%fused_computation.24 | convolution fusion | flops 4845600768 | bytes 11810816 | tf_op jit(solution)/shard_map/dot_general | solution.py:257
  59.8 0.0 copy-start.4
  59.8 0.0 copy-start.6
  59.8 0.2 convert_multiply_fusion.8
  60.0 2.4 collective-permute-start
  62.5 0.0 copy-done.4
  62.5 0.8 slice_bitcast_fusion.3
  63.3 0.0 copy-done.6
  63.3 0.1 slice.168
  63.3 0.5 collective-permute-done
  63.9 1.5 fusion.47
  65.3 63.2 %shard_map.74 = (bf16[2048,768]{1,0:T(8,128)(2,1)}, bf16[1536,2048]{1,0:T(8,128)(2,1)}) custom-call(bf16[128,512]{1,0:T(8,128)(2,1)} %get-tuple-element.24.down, bf16[256,768]{1,0:T(8,128)(2,1)} %get-tuple-element.22.weight, bf16[1536,256]{1,0:T(8,128)(2,1)} %bitcast.52), custom_call_target="tpu_custom_call" | custom-call | tf_op jit(solution)/shard_map/pallas_call | solution.py:213
  128.6 0.0 copy-start.2
  128.6 4.2 %fusion.3 = f32[1536]{0:T(1024)S(1)} fusion(bf16[1536,2048]{1,0:T(8,128)(2,1)} %get-tuple-element.15), kind=kLoop, calls=%fused_computation.9 | loop fusion | flops 9435648 | bytes 6297600 | tf_op jit(solution)/shard_map/reduce_sum | solution.py:233
  132.8 0.3 copy-done.2
  133.2 7.5 %fusion.24 = bf16[1536,768]{1,0:T(8,128)(2,1)S(1)} fusion(bf16[2048,768]{1,0:T(8,128)(2,1)} %get-tuple-element.16, bf16[1536,2048]{1,0:T(8,128)(2,1)S(1)} %copy-done.2, f32[2048]{0:T(1024)S(1)} %bitcast.57, f32[1536]{0:T(1024)S(1)} %add_rsqrt_fusion.1), kind=kOutput, calls=%fused_computation.25 | convolution fusion | flops 4845600768 | bytes 11810816 | tf_op jit(solution)/shard_map/dot_general | solution.py:257
  140.7 0.2 convert_multiply_fusion.7
  140.9 3.2 %collective-permute-start.1 = (f32[6,2,256]{2,1,0:T(2,128)S(1)}, f32[6,2,256]{2,1,0:T(2,128)S(1)}, u32[]{:S(2)}, u32[]{:S(2)}) collective-permute-start(f32[6,2,256]{2,1,0:T(2,128)S(1)} %slice.177), channel_id=1, source_target_pairs={{0,4},{4,8},{8,12},{12,16},{16,20},{20,24},{24,28},{1,5},{5,9},{9,... | collective-permute-start | bytes 36872 | tf_op jit(solution)/shard_map/ppermute | solution.py:228
  144.1 0.1 slice.174
  144.2 1.1 collective-permute-done.1
  145.3 1.5 fusion.41
  146.8 63.3 %shard_map.75 = (bf16[2048,768]{1,0:T(8,128)(2,1)}, bf16[1536,2048]{1,0:T(8,128)(2,1)}) custom-call(bf16[128,512]{1,0:T(8,128)(2,1)} %get-tuple-element.26.down, bf16[256,768]{1,0:T(8,128)(2,1)} %get-tuple-element.23.weight, bf16[1536,256]{1,0:T(8,128)(2,1)} %bitcast.49), custom_call_target="tpu_custom_call" | custom-call | tf_op jit(solution)/shard_map/pallas_call | solution.py:213
  210.1 0.0 copy-start.1
  210.1 4.2 %fusion.6 = f32[1536]{0:T(1024)S(1)} fusion(bf16[1536,2048]{1,0:T(8,128)(2,1)} %get-tuple-element.17), kind=kLoop, calls=%fused_computation.12 | loop fusion | flops 9435648 | bytes 6297600 | tf_op jit(solution)/shard_map/reduce_sum | solution.py:233
  214.3 0.3 copy-done.1
  214.7 7.5 %fusion.27 = bf16[1536,768]{1,0:T(8,128)(2,1)S(1)} fusion(bf16[2048,768]{1,0:T(8,128)(2,1)} %get-tuple-element.18, bf16[1536,2048]{1,0:T(8,128)(2,1)S(1)} %copy-done.1, f32[2048]{0:T(1024)S(1)} %bitcast.56, f32[1536]{0:T(1024)S(1)} %add_rsqrt_fusion), kind=kOutput, calls=%fused_computation.26 | convolution fusion | flops 4845600768 | bytes 11810816 | tf_op jit(solution)/shard_map/dot_general | solution.py:257
  222.2 0.2 convert_multiply_fusion.6
  222.4 2.5 collective-permute-start.2
  224.9 0.1 slice.180
  225.0 1.3 collective-permute-done.2
  226.3 1.5 fusion.35
  227.8 23.8 %shard_map.76 = (bf16[1024,512]{1,0:T(8,128)(2,1)}, bf16[1536,1024]{1,0:T(8,128)(2,1)}) custom-call(bf16[128,512]{1,0:T(8,128)(2,1)} %get-tuple-element.25.weight, bf16[1536,256]{1,0:T(8,128)(2,1)} %bitcast.54), custom_call_target="tpu_custom_call" | custom-call | tf_op jit(solution)/shard_map/pallas_call | solution.py:199
  251.6 5.6 %fusion.52 = f32[1536,512]{1,0:T(8,128)} fusion(bf16[1536,1024]{1,0:T(8,128)(2,1)} %get-tuple-element.19, bf16[1024,512]{1,0:T(8,128)(2,1)} %get-tuple-element.20), kind=kOutput, calls=%fused_computation.82 | convolution fusion | flops 1610612736 | bytes 7340032 | tf_op jit(solution)/shard_map/dot_general | solution.py:273
  (9 shorter events, 0.1 us)
Async XLA Ops:
  0.0 2.1 copy-start.3
  3.2 48.8 %copy-start.5 = (f32[3,2048]{1,0:T(4,128)S(1)}, f32[3,2048]{1,0:T(4,128)}, u32[]{:S(2)}) copy-start(f32[3,2048]{1,0:T(4,128)} %param.8) | copy-start | bytes 73732
  47.7 4.6 %copy-start = (bf16[1536,2048]{1,0:T(8,128)(2,1)S(1)}, bf16[1536,2048]{1,0:T(8,128)(2,1)}, u32[]{:S(2)}) copy-start(bf16[1536,2048]{1,0:T(8,128)(2,1)} %get-tuple-element.13) | copy-start | bytes 18874372
  59.8 2.7 %copy-start.4 = (bf16[3,128,512]{2,1,0:T(8,128)(2,1)S(1)}, bf16[3,128,512]{2,1,0:T(8,128)(2,1)}, u32[]{:S(2)}) copy-start(bf16[3,128,512]{2,1,0:T(8,128)(2,1)} %param.13) | copy-start | bytes 1179652
  59.8 3.4 %copy-start.6 = (bf16[3,3,256]{2,1,0:T(4,128)(2,1)S(1)}, bf16[3,3,256]{2,1,0:T(4,128)(2,1)}, u32[]{:S(2)}) copy-start(bf16[3,3,256]{2,1,0:T(4,128)(2,1)} %param.12) | copy-start | bytes 13828
  60.0 3.8 %collective-permute-start = (f32[6,2,256]{2,1,0:T(2,128)S(1)}, f32[6,2,256]{2,1,0:T(2,128)S(1)}, u32[]{:S(2)}, u32[]{:S(2)}) collective-permute-start(f32[6,2,256]{2,1,0:T(2,128)S(1)} %slice.171), channel_id=1, source_target_pairs={{0,4},{4,8},{8,12},{12,16},{16,20},{20,24},{24,28},{1,5},{5,9},{9,... | collective-permute-start | bytes 36872 | tf_op jit(solution)/shard_map/ppermute | solution.py:228
  128.6 4.6 %copy-start.2 = (bf16[1536,2048]{1,0:T(8,128)(2,1)S(1)}, bf16[1536,2048]{1,0:T(8,128)(2,1)}, u32[]{:S(2)}) copy-start(bf16[1536,2048]{1,0:T(8,128)(2,1)} %get-tuple-element.15) | copy-start | bytes 18874372
  140.9 4.4 %collective-permute-start.1 = (f32[6,2,256]{2,1,0:T(2,128)S(1)}, f32[6,2,256]{2,1,0:T(2,128)S(1)}, u32[]{:S(2)}, u32[]{:S(2)}) collective-permute-start(f32[6,2,256]{2,1,0:T(2,128)S(1)} %slice.177), channel_id=1, source_target_pairs={{0,4},{4,8},{8,12},{12,16},{16,20},{20,24},{24,28},{1,5},{5,9},{9,... | collective-permute-start | bytes 36872 | tf_op jit(solution)/shard_map/ppermute | solution.py:228
  210.1 4.6 %copy-start.1 = (bf16[1536,2048]{1,0:T(8,128)(2,1)S(1)}, bf16[1536,2048]{1,0:T(8,128)(2,1)}, u32[]{:S(2)}) copy-start(bf16[1536,2048]{1,0:T(8,128)(2,1)} %get-tuple-element.17) | copy-start | bytes 18874372
  222.4 3.9 %collective-permute-start.2 = (f32[6,2,256]{2,1,0:T(2,128)S(1)}, f32[6,2,256]{2,1,0:T(2,128)S(1)}, u32[]{:S(2)}, u32[]{:S(2)}) collective-permute-start(f32[6,2,256]{2,1,0:T(2,128)S(1)} %slice.183), channel_id=1, source_target_pairs={{0,4},{4,8},{8,12},{12,16},{16,20},{20,24},{24,28},{1,5},{5,9},{9,... | collective-permute-start | bytes 36872 | tf_op jit(solution)/shard_map/ppermute | solution.py:228

commit v3 on v2

--- a/solution.py
+++ b/solution.py
@@ -158,11 +158,58 @@
         each.drain()
 
 
-def boundary_kernel(sizes, pieces, down, weight, mixer, weight_out, acts_out, down_all, mix_all, acts, *sems):
+def project(chunks, weights, gain, acts_all, weight_all, normed, gates):
+    rows = chunks[0].shard.shape[0]
+    group = 16 if rows % 16 == 0 else rows
+
+    def norm(i):
+        chunks[i].complete()
+
+        @pl.loop(0, rows // group)
+        def _(j):
+            cut = pl.ds(pl.multiple_of(i * rows + j * group, group), group)
+            values = acts_all[cut, :].astype(jnp.float32)
+            scale = lax.rsqrt(jnp.mean(values * values, axis=-1, keepdims=True) + epsilon)
+            normed[cut, :] = (values * scale * gain[...]).astype(normed.dtype)
+
+    def multiply(i):
+        cut = pl.ds(i * rows, rows)
+        gates[cut, :] = jnp.dot(
+            normed[cut, :], weight_all[...], preferred_element_type=jnp.float32
+        ).astype(gates.dtype)
+
+    def take(i):
+        for act in chunks[i].steps():
+            act()
+        norm(i)
+
+    early = max(len(chunks) - 2, 0)
+    alternate([functools.partial(take, i) for i in range(early)], weights.steps())
+    weights.complete()
+    for i in range(early):
+        multiply(i)
+    for i in range(early, len(chunks)):
+        take(i)
+        multiply(i)
+
+
+def first_kernel(sizes, pieces, weight, acts, gain, gates, weight_all, acts_all, normed, *sems):
+    weights = Gather("sp", sizes[0], 0, weight, weight_all, sems[:6])
+    chunks = cut_up("tp", sizes[1], pieces, acts, acts_all, sems[6:])
+    greet([weights, chunks[0]])
+    weights.start()
+    for chunk in chunks:
+        chunk.start()
+    project(chunks, weights, gain, acts_all, weight_all, normed, gates)
+    for each in chunks + [weights]:
+        each.drain()
+
+
+def boundary_kernel(sizes, pieces, down, weight, mixer, gain, gates, weight_all, acts_all, normed, down_all, mix_all, acts, *sems):
     downs = Gather("sp", sizes[0], 0, down, down_all, sems[:6])
-    weights = Gather("sp", sizes[0], 0, weight, weight_out, sems[6:12])
+    weights = Gather("sp", sizes[0], 0, weight, weight_all, sems[6:12])
     mixes = cut_up("tp", sizes[1], pieces, mixer, mix_all, sems[12 : 12 + 6 * pieces])
-    chunks = cut_up("tp", sizes[1], pieces, acts, acts_out, sems[12 + 6 * pieces :])
+    chunks = cut_up("tp", sizes[1], pieces, acts, acts_all, sems[12 + 6 * pieces :])
     rows = mixer.shape[0] // pieces
     greet([downs, mixes[0]])
     downs.start()
@@ -181,9 +228,7 @@
             mix_all[cut, :], down_all[...], preferred_element_type=jnp.float32
         ).astype(acts.dtype)
         chunks[i].start()
-    alternate([act for chunk in chunks for act in chunk.steps()], weights.steps())
-    for each in chunks + [weights]:
-        each.complete()
+    project(chunks, weights, gain, acts_all, weight_all, normed, gates)
     for each in [downs] + mixes + chunks + [weights]:
         each.drain()
 
@@ -206,32 +251,43 @@
     )(weight, acts)
 
 
-def cross_boundary(down, weight, mixer, pieces, number):
+def begin(weight, acts, gain, pieces, number):
+    sizes = lax.axis_size("sp"), lax.axis_size("tp")
+    weight_all, acts_all = grown(weight, 0, sizes[0]), grown(acts, 1, sizes[1])
+    return pl.pallas_call(
+        functools.partial(first_kernel, sizes, pieces),
+        out_shape=jax.ShapeDtypeStruct((acts.shape[0], weight.shape[1]), acts.dtype),
+        in_specs=[pl.BlockSpec(memory_space=pltpu.VMEM)] * 3,
+        out_specs=pl.BlockSpec(memory_space=pltpu.VMEM),
+        scratch_shapes=[pltpu.VMEM(a.shape, a.dtype) for a in (weight_all, acts_all, acts_all)]
+        + sems_of(sizes[0])
+        + sems_of(sizes[1], pieces),
+        compiler_params=pltpu.CompilerParams(collective_id=number, has_side_effects=True),
+    )(weight, acts, gain)
+
+
+def cross_boundary(down, weight, mixer, gain, pieces, number):
     sizes = lax.axis_size("sp"), lax.axis_size("tp")
     acts = jax.ShapeDtypeStruct((mixer.shape[0], down.shape[1]), mixer.dtype)
     down_all, mix_all = grown(down, 0, sizes[0]), grown(mixer, 1, sizes[1])
+    weight_all, acts_all = grown(weight, 0, sizes[0]), grown(acts, 1, sizes[1])
+    held = weight_all, acts_all, acts_all, down_all, mix_all, acts
     return pl.pallas_call(
         functools.partial(boundary_kernel, sizes, pieces),
-        out_shape=(grown(weight, 0, sizes[0]), grown(acts, 1, sizes[1])),
-        in_specs=[pl.BlockSpec(memory_space=pltpu.VMEM)] * 3,
-        out_specs=(pl.BlockSpec(memory_space=pl.ANY),) * 2,
-        scratch_shapes=[pltpu.VMEM(a.shape, a.dtype) for a in (down_all, mix_all, acts)]
+        out_shape=jax.ShapeDtypeStruct((mixer.shape[0], weight.shape[1]), mixer.dtype),
+        in_specs=[pl.BlockSpec(memory_space=pltpu.VMEM)] * 4,
+        out_specs=pl.BlockSpec(memory_space=pltpu.VMEM),
+        scratch_shapes=[pltpu.VMEM(a.shape, a.dtype) for a in held]
         + sems_of(sizes[0], 2)
         + sems_of(sizes[1], 2 * pieces),
         compiler_params=pltpu.CompilerParams(collective_id=number, has_side_effects=True),
-    )(down, weight, mixer)
+    )(down, weight, mixer, gain)
 
 
 def from_behind(block, axis, distance):
     devices = range(lax.axis_size(axis))
     route = [(i - distance, i) for i in devices if i - distance in devices]
     return lax.ppermute(block, axis, route)
-
-
-def normalize(values_in, gain_row):
-    values = values_in.astype(jnp.float32)
-    scale = lax.rsqrt(jnp.mean(values * values, axis=-1, keepdims=True) + epsilon)
-    return (values * scale * gain_row.astype(jnp.float32)).astype(jnp.bfloat16)
 
 
 def convolve(extended, taps):
@@ -249,12 +305,9 @@
     sequences, rows, width = tokens.shape
     channels = weight_outer.shape[2]
     weight_in = jnp.concatenate([weight_outer, weight_inner, weight_value], axis=2)
-    joined, whole = gather_both(
-        weight_in[0], tokens.reshape(sequences * rows, width), sequences, 0
-    )
+    tokens = tokens.reshape(sequences * rows, width)
+    gates = begin(weight_in[0], tokens, norm_gains[:1], sequences, 0)
     for layer in range(layers):
-        normed = normalize(whole, norm_gains[layer])
-        gates = jnp.dot(normed, joined, preferred_element_type=jnp.float32).astype(jnp.bfloat16)
         outer, inner, value = (
             gates[:, i * channels : (i + 1) * channels].reshape(sequences, rows, channels)
             for i in range(3)
@@ -266,8 +319,10 @@
         mixer = (outer.astype(jnp.float32) * conved).astype(jnp.bfloat16)
         mixer = mixer.reshape(sequences * rows, channels)
         if layer < layers - 1:
-            joined, whole = cross_boundary(
-                weight_output[layer], weight_in[layer + 1], mixer, sequences, layer + 1
+            following = layer + 1
+            gain = norm_gains[following : following + 1]
+            gates = cross_boundary(
+                weight_output[layer], weight_in[following], mixer, gain, sequences, following
             )
     down, full_mix = gather_both(weight_output[layers - 1], mixer, sequences, layers)
     result = jnp.dot(full_mix, down, preferred_element_type=jnp.float32)

time: 258 us -> 277 us (1.074)
  Pallas kernels: 195 us -> 246 us
  matrix products: 28.2 us -> 5.64 us
  other arithmetic: 17.7 us -> 9.19 us
    pallas_call x0 -> x1, Pallas kernels: none -> 62.8 us  [begin(): pl.pallas_call(functools.partial(first_kernel, sizes, pieces), out_shape=...]
    pallas_call x2 -> x1, Pallas kernels: 68.3 us -> 23.7 us  [gather_both(): pl.pallas_call(functools.partial(gather_kernel, sizes, pieces), out_shape...]
    pallas_call x2, Pallas kernels: 127 us -> 160 us  [cross_boundary(): pl.pallas_call(functools.partial(boundary_kernel, sizes, pieces), out_sha...]
    dot_general x3 -> x0, matrix products: 22.5 us -> none  [local(): jnp.dot(normed, joined, preferred_element_type=jnp.float32)]
    reduce_sum x3 -> x0, other arithmetic: 12.7 us -> none  [normalize(): jnp.mean(values * values, axis=-1, keepdims=True) + epsilon]
    mul x3, other arithmetic: 0.47 us -> 4.71 us  [local(): gated = inner.astype(jnp.float32) * value.astype(jnp.float32)]
where the time goes in v3:
time: 277 us
  Pallas kernels  246 us (89%)
  other arithmetic  9.19 us (3%)
  starting transfers between devices  6.68 us (2%)
  matrix products  5.64 us (2%)
  local copies, waits for them, and re-layouts  5.43 us (2%)
  waiting for transfers between devices  3.37 us (1%)
    pallas_call x2, Pallas kernels, cross_boundary(): pl.pallas_call(functools.partial(boundary_kernel, sizes, pieces), out_sha...  160 us
    pallas_call x1, Pallas kernels, begin(): pl.pallas_call(functools.partial(first_kernel, sizes, pieces), out_shape=...  62.8 us
    pallas_call x1, Pallas kernels, gather_both(): pl.pallas_call(functools.partial(gather_kernel, sizes, pieces), out_shape...  23.7 us
    ppermute x3, starting transfers between devices, from_behind(): return lax.ppermute(block, axis, route)  6.68 us
    dot_general x1, matrix products, local(): result = jnp.dot(full_mix, down, preferred_element_type=jnp.float32)  5.64 us
  transfers between devices with their start and end apart: 3, of which 3 were waited for; matrix products, arithmetic and copies ran while one was open for 0% of the time, Pallas kernels for 0%

profile of v3, /device:TPU:0, one launch (start us, length us, event | category | flops | bytes accessed | tf_op | source)
XLA Modules:
  0.0 276.9 jit_solution(5645439165169627729)
XLA Ops:
  0.0 0.0 copy-start
  0.0 1.5 fusion.21
  1.5 1.0 constant_dynamic-update-slice_fusion.2
  2.5 1.0 constant_dynamic-update-slice_fusion.1
  3.6 0.0 copy-done
  3.6 1.0 slice_bitcast_fusion
  4.6 62.8 %shard_map.73 = bf16[1536,768]{1,0:T(8,128)(2,1)} custom-call(bf16[256,768]{1,0:T(8,128)(2,1)} %get-tuple-element.9.weight, bf16[1536,512]{1,0:T(8,128)(2,1)} %bitcast.49, f32[1,2048]{1,0:T(1,128)} %get-tuple-element.16.gain), custom_call_target="tpu_custom_call" | custom-call | tf_op jit(solution)/shard_map/pallas_call | solution.py:257
  67.4 0.0 copy-start.1
  67.4 0.0 copy-start.2
  67.5 1.6 convert_multiply_fusion.2
  69.1 0.0 slice-start
  69.1 2.5 collective-permute-start
  71.6 0.0 copy-done.1
  71.6 0.8 slice_bitcast_fusion.3
  72.4 0.0 copy-done.2
  72.4 0.6 collective-permute-done
  73.0 0.0 slice-done
  73.0 1.5 fusion.17
  74.5 79.7 %shard_map.74 = bf16[1536,768]{1,0:T(8,128)(2,1)} custom-call(bf16[128,512]{1,0:T(8,128)(2,1)} %get-tuple-element.12.down, bf16[256,768]{1,0:T(8,128)(2,1)} %get-tuple-element.10.weight, bf16[1536,256]{1,0:T(8,128)(2,1)} %bitcast.47, f32[1,2048]{1,0:T(1,128)} %get-tuple-element.17.gain), custom_call_target="tpu_custom_call" | custom-call | tf_op jit(solution)/shard_map/pallas_call | solution.py:275
  154.2 1.6 convert_multiply_fusion.1
  155.8 0.0 slice-start.1
  155.8 2.3 collective-permute-start.1
  158.1 1.4 collective-permute-done.1
  159.5 0.0 slice-done.1
  159.5 1.5 fusion.11
  160.9 80.2 %shard_map.75 = bf16[1536,768]{1,0:T(8,128)(2,1)} custom-call(bf16[128,512]{1,0:T(8,128)(2,1)} %get-tuple-element.14.down, bf16[256,768]{1,0:T(8,128)(2,1)} %get-tuple-element.11.weight, bf16[1536,256]{1,0:T(8,128)(2,1)} %bitcast.46, f32[1,2048]{1,0:T(1,128)} %get-tuple-element.15.gain), custom_call_target="tpu_custom_call" | custom-call | tf_op jit(solution)/shard_map/pallas_call | solution.py:275
  241.2 1.6 convert_multiply_fusion
  242.7 0.0 slice-start.2
  242.8 1.9 collective-permute-start.2
  244.7 1.4 collective-permute-done.2
  246.0 0.0 slice-done.2
  246.1 1.5 fusion.5
  247.5 23.7 %shard_map.76 = (bf16[1024,512]{1,0:T(8,128)(2,1)}, bf16[1536,1024]{1,0:T(8,128)(2,1)}) custom-call(bf16[128,512]{1,0:T(8,128)(2,1)} %get-tuple-element.13.weight, bf16[1536,256]{1,0:T(8,128)(2,1)} %bitcast.48), custom_call_target="tpu_custom_call" | custom-call | tf_op jit(solution)/shard_map/pallas_call | solution.py:244
  271.2 5.6 %fusion.22 = f32[1536,512]{1,0:T(8,128)} fusion(bf16[1536,1024]{1,0:T(8,128)(2,1)} %get-tuple-element.7, bf16[1024,512]{1,0:T(8,128)(2,1)} %get-tuple-element.8), kind=kOutput, calls=%fused_computation.52 | convolution fusion | flops 1610612736 | bytes 7340032 | tf_op jit(solution)/shard_map/dot_general | solution.py:328
  (5 shorter events, 0.1 us)
Async XLA Ops:
  0.0 3.6 %copy-start = (bf16[3,256,256]{2,1,0:T(8,128)(2,1)S(1)}, bf16[3,256,256]{2,1,0:T(8,128)(2,1)}, u32[]{:S(2)}) copy-start(bf16[3,256,256]{2,1,0:T(8,128)(2,1)} %param.11) | copy-start | bytes 1179652
  67.4 4.2 %copy-start.1 = (bf16[3,128,512]{2,1,0:T(8,128)(2,1)S(1)}, bf16[3,128,512]{2,1,0:T(8,128)(2,1)}, u32[]{:S(2)}) copy-start(bf16[3,128,512]{2,1,0:T(8,128)(2,1)} %param.13) | copy-start | bytes 1179652
  67.4 5.0 %copy-start.2 = (bf16[3,3,256]{2,1,0:T(4,128)(2,1)S(1)}, bf16[3,3,256]{2,1,0:T(4,128)(2,1)}, u32[]{:S(2)}) copy-start(bf16[3,3,256]{2,1,0:T(4,128)(2,1)} %param.12) | copy-start | bytes 13828
  69.1 4.0 %slice-start = ((bf16[1536,768]{1,0:T(8,128)(2,1)}), bf16[1536,256]{1,0:T(8,128)(2,1)S(1)}, s32[]{:S(2)}) async-start(bf16[1536,768]{1,0:T(8,128)(2,1)} %shard_map.73), calls=%async_computation | async-start | bytes 1572864 | tf_op jit(solution)/shard_map/slice | solution.py:312
  69.1 3.9 %collective-permute-start = (f32[6,2,256]{2,1,0:T(2,128)S(1)}, f32[6,2,256]{2,1,0:T(2,128)S(1)}, u32[]{:S(2)}, u32[]{:S(2)}) collective-permute-start(f32[6,2,256]{2,1,0:T(2,128)S(1)} %slice.168), channel_id=1, source_target_pairs={{0,4},{4,8},{8,12},{12,16},{16,20},{20,24},{24,28},{1,5},{5,9},{9,... | collective-permute-start | bytes 36872 | tf_op jit(solution)/shard_map/ppermute | solution.py:290
  155.8 3.7 %slice-start.1 = ((bf16[1536,768]{1,0:T(8,128)(2,1)}), bf16[1536,256]{1,0:T(8,128)(2,1)S(1)}, s32[]{:S(2)}) async-start(bf16[1536,768]{1,0:T(8,128)(2,1)} %shard_map.74), calls=%async_computation.1 | async-start | bytes 1572864 | tf_op jit(solution)/shard_map/slice | solution.py:312
  155.8 3.6 %collective-permute-start.1 = (f32[6,2,256]{2,1,0:T(2,128)S(1)}, f32[6,2,256]{2,1,0:T(2,128)S(1)}, u32[]{:S(2)}, u32[]{:S(2)}) collective-permute-start(f32[6,2,256]{2,1,0:T(2,128)S(1)} %slice.171), channel_id=1, source_target_pairs={{0,4},{4,8},{8,12},{12,16},{16,20},{20,24},{24,28},{1,5},{5,9},{9,... | collective-permute-start | bytes 36872 | tf_op jit(solution)/shard_map/ppermute | solution.py:290
  242.7 3.3 %slice-start.2 = ((bf16[1536,768]{1,0:T(8,128)(2,1)}), bf16[1536,256]{1,0:T(8,128)(2,1)S(1)}, s32[]{:S(2)}) async-start(bf16[1536,768]{1,0:T(8,128)(2,1)} %shard_map.75), calls=%async_computation.2 | async-start | bytes 1572864 | tf_op jit(solution)/shard_map/slice | solution.py:312
  242.8 3.3 %collective-permute-start.2 = (f32[6,2,256]{2,1,0:T(2,128)S(1)}, f32[6,2,256]{2,1,0:T(2,128)S(1)}, u32[]{:S(2)}, u32[]{:S(2)}) collective-permute-start(f32[6,2,256]{2,1,0:T(2,128)S(1)} %slice.174), channel_id=1, source_target_pairs={{0,4},{4,8},{8,12},{12,16},{16,20},{20,24},{24,28},{1,5},{5,9},{9,... | collective-permute-start | bytes 36872 | tf_op jit(solution)/shard_map/ppermute | solution.py:290
